TPU v7x, 128 devices: a whole 4x4x4 slice. The times are simulated.
128 devices in a mesh: fs: 16 (over z, y), rep: 4 (over x), tp: 2 (over core).
Axes of the slice: x: 4, y: 4, z: 4, core: 2. Of those that a mesh axis runs over, the one named last changes fastest.
Arguments:
- saved_latent: bfloat16 [49152, 2048], P(('fs', 'rep')), may hold values from -6 to 6
- query_cotangent: bfloat16 [49152, 3072], P(('fs', 'rep'), 'tp'), may hold values from -6 to 6
- mix_cotangent: bfloat16 [49152, 4096], P(('fs', 'rep')), may hold values from -6 to 6
- head_outputs: bfloat16 [49152, 2048], P(('fs', 'rep'), 'tp'), may hold values from -6 to 6
- query_weight: float32 [2048, 3072], P('fs', 'tp'), may hold values from -0.125 to 0.125
- out_weight: float32 [4096, 2048], P('fs', 'tp'), may hold values from -0.125 to 0.125
- query_basis: bfloat16 [2048, 256], replicated, may hold values from -0.125 to 0.125
- out_basis: bfloat16 [4096, 256], replicated, may hold values from -0.09375 to 0.09375
- query_mean: float32 [256, 3072], P('fs', 'tp'), may hold values from -3 to 3
- query_var: float32 [256, 3072], P('fs', 'tp'), may hold values from 0.1 to 1
- out_mean: float32 [256, 2048], P('fs', 'tp'), may hold values from -3 to 3
- out_var: float32 [256, 2048], P('fs', 'tp'), may hold values from 0.1 to 1
Outputs:
- query_step: float32 [2048, 3072], P('fs', 'tp')
- out_step: float32 [4096, 2048], P('fs', 'tp')
- query_copy: bfloat16 [2048, 3072], P('fs', 'tp')
- out_copy: bfloat16 [4096, 2048], P('fs', 'tp')
All inputs are finite; a program needn't handle non-finite values.
Results may differ from a plain program's by a relative error of at most 0.001.
Values sent between devices are 32-bit elements; how exact they have to be, the bound alone decides.
No kernel may reach another device: no remote copies, remote signals or barrier semaphores. Data moves between devices by JAX's collectives and lax.ppermute only.
A program may use at most 128 MiB of HBM per device.

v0:
```python
import functools

import jax
import jax.numpy as jnp
from jax import lax
from jax.experimental import pallas as pl
from jax.experimental.pallas import tpu as pltpu
from jax.sharding import PartitionSpec as P


F32 = jnp.float32
BF16 = jnp.bfloat16
AXES = ("fs", "rep", "tp")
RING = 4
FAR = 16
FRONT = 51
STEPS = 4
AHEAD = 24
ORDERS = ((4, 2, 1), (2, 1, 4))


def first(place, core):
    gray, top = (place // 2) ^ (place % 2), place // 2
    return gray + core * (top - gray)


def second(place, core):
    return first(place, 1 - core)


def place_of(one, two, core):
    return 2 * (two + core * (one - two)) + (one ^ two)


def devices():
    return [(z, y, x, c) for z in range(RING) for y in range(RING) for x in range(RING) for c in range(2)]


def number(z, y, x, core):
    return ((z * RING + y) * RING + x) * 2 + core


def partners(phase, offset):
    pairs = []
    for *spots, core in devices():
        bits = (offset & 1, (offset >> 1) & 1, offset >> 2)
        there = []
        for spot, bit in zip(spots, bits):
            one, two = first(spot, core), second(spot, core)
            there.append(place_of(one ^ bit, two, core) if phase == 1 else place_of(one, two ^ bit, core))
        pairs.append((number(*spots, core), number(*there, core)))
    return pairs


def first_groups():
    groups = {}
    for z, y, x, core in devices():
        key = tuple(second(s, core) for s in (x, y, z)) + (core,)
        slot = sum(first(s, core) << k for s, k in ((x, 2), (y, 1), (z, 0)))
        groups.setdefault(key, {})[slot] = number(z, y, x, core)
    return [[g[s] for s in range(8)] for g in groups.values()]


def here():
    block = lax.axis_index("fs")
    return block // RING, block % RING, lax.axis_index("rep"), lax.axis_index("tp")


def halves(value):
    high = value.astype(BF16)
    return high, (value - high.astype(F32)).astype(BF16)


def params(mebibytes):
    return pltpu.CompilerParams(vmem_limit_bytes=mebibytes << 20)


def cost(micros):
    return pl.CostEstimate(flops=int(micros * 1e8), bytes_accessed=int(micros * 1e6), transcendentals=0)


def part_of(flip):
    def index(i):
        _, _, x, core = here()
        return place_of(first(x, core) ^ flip, i, core)

    return index


def rows_of(spot, pair):
    z, y, _, core = here()
    there_y = place_of(first(y, core) ^ (spot >> 1), pair >> 1, core)
    there_z = place_of(first(z, core) ^ (spot & 1), pair & 1, core)
    return there_z * RING + there_y


def spread_rows(rows, qterm, oterm, outs, base):
    width = qterm.shape[1]
    for spot in range(4):
        for pair in range(4):
            at = pl.ds(pl.multiple_of(rows_of(spot, pair) * rows, rows), rows)
            outs[spot][base + pair, :, :width] = qterm[at, :]
            outs[spot][base + pair, :, width:] = oterm[at, :]


def over_tokens(low, other):
    value = jnp.dot(low[0], other, preferred_element_type=F32)
    return value + jnp.dot(low[1], other, preferred_element_type=F32)


def blocks_kernel(rows, flip, qlow, olow, cot, heads, outs, qterm, oterm):
    for part in range(2):
        index = part_of(flip)(part)
        for low, other, term in ((qlow, cot, qterm), (olow, heads, oterm)):
            width = term.shape[1]
            at = pl.ds(pl.multiple_of(index * width, 128), width)
            term[...] = over_tokens(low, other[:, at])
        spread_rows(rows, qterm, oterm, outs, 4 * part)


def front_kernel(rows, latent, mix, qbasis, obasis, cot, heads, *refs):
    qlow, olow, outs = refs[0], refs[1], refs[2:6]
    xs, ms, qs, os, qfar, ofar, total, qterm, oterm, sems = refs[6:]
    copies, waits = [], {}

    def bring(key, source, target):
        waits.setdefault(key, []).append(len(copies))
        copies.append(pltpu.make_async_copy(source, target, sems.at[len(copies)]))

    for name, tokens, basis, inside, beside in (("m", mix, obasis, ms, os), ("x", latent, qbasis, xs, qs)):
        wide = tokens.shape[1] // STEPS
        for k in range(STEPS):
            at = pl.ds(k * wide, wide)
            bring((name, k), basis.at[at, :], beside.at[at, :])
            bring((name, k), tokens.at[:, at], inside.at[:, at])
    for source, target in ((cot, qfar), (heads, ofar)):
        width = target.shape[2]
        for part in range(2):
            at = pl.ds(pl.multiple_of(part_of(1)(part) * width, 128), width)
            bring(part, source.at[:, at], target.at[part])
    begun = 0

    def ahead(upto):
        nonlocal begun
        while begun < min(upto, len(copies)):
            copies[begun].start()
            begun += 1

    def ready(key):
        for k in waits[key]:
            copies[k].wait()
        ahead(max(waits[key]) + 1 + AHEAD)

    apart = lax.axis_index("fs") >= 0
    ahead(AHEAD)
    for name, inside, beside, low in (("m", ms, os, olow), ("x", xs, qs, qlow)):
        wide = inside.shape[1] // STEPS
        for k in range(STEPS):

            @pl.when(apart)
            def _():
                ready((name, k))
                term = jnp.dot(
                    inside[:, k * wide : (k + 1) * wide],
                    beside[k * wide : (k + 1) * wide, :],
                    preferred_element_type=F32,
                )
                if k > 0:
                    term += total[...]
                if k < STEPS - 1:
                    total[...] = term
                else:
                    high, rest = halves(term)
                    low[0] = high.T
                    low[1] = rest.T

    for part in range(2):

        @pl.when(apart)
        def _():
            ready(part)
            qterm[...] = over_tokens(qlow, qfar[part])
            oterm[...] = over_tokens(olow, ofar[part])
            spread_rows(rows, qterm, oterm, outs, 4 * part)


def front(latent, mix, qbasis, obasis, cot, heads):
    tokens, rank = latent.shape[0], qbasis.shape[1]
    rows = rank // (RING * RING)
    qwide, owide = cot.shape[1] // RING, heads.shape[1] // RING
    low = jax.ShapeDtypeStruct((2, rank, tokens), BF16)
    kept = [jax.ShapeDtypeStruct((2, tokens, w), BF16) for w in (qwide, owide)]
    block = jax.ShapeDtypeStruct((8, rows, qwide + owide), F32)
    return pl.pallas_call(
        functools.partial(front_kernel, rows),
        in_specs=[pl.BlockSpec(memory_space=pltpu.HBM)] * 6,
        out_shape=[low, low] + [block] * 4,
        scratch_shapes=[pltpu.VMEM(a.shape, BF16) for a in (latent, mix, qbasis, obasis, *kept)]
        + [pltpu.VMEM((tokens, rank), F32)]
        + [pltpu.VMEM((rank, w), F32) for w in (qwide, owide)]
        + [pltpu.SemaphoreType.DMA((4 * STEPS + 4,))],
        compiler_params=params(FRONT),
        cost_estimate=cost(7),
        name="front",
    )(latent, mix, qbasis, obasis, cot, heads)


def near_kernel(rows, qlow, olow, cot, heads, *refs):
    blocks_kernel(rows, 0, qlow, olow, cot, heads, refs[:4], *refs[4:])


def near_blocks(qlow, olow, cot, heads):
    rank = qlow.shape[1]
    rows = rank // (RING * RING)
    qwide, owide = cot.shape[1] // RING, heads.shape[1] // RING
    block = jax.ShapeDtypeStruct((8, rows, qwide + owide), F32)
    return pl.pallas_call(
        functools.partial(near_kernel, rows),
        out_shape=[block] * 4,
        scratch_shapes=[pltpu.VMEM((rank, w), F32) for w in (qwide, owide)],
        compiler_params=params(FAR),
        cost_estimate=cost(2),
        name="near",
    )(qlow, olow, cot, heads)


def tree(values):
    while len(values) > 1:
        values = [a + b for a, b in zip(values[::2], values[1::2])]
    return values[0]


def lanes(value):
    _, wide = value.shape
    total = jnp.sum(value, axis=0, keepdims=True)
    return sum(total[:, k : k + 128] for k in range(0, wide, 128))


def total_kernel(*refs):
    value = tree([r[...] for r in refs[:8]])
    for half in range(2):
        refs[8 + half][...] = value[4 * half : 4 * half + 4]


def squares_kernel(split, *refs):
    proj, squares = refs[4:]
    for half in range(2):
        proj[4 * half : 4 * half + 4] = refs[2 * half][...] + refs[2 * half + 1][...]
    value = proj[...]
    value = value.reshape(value.shape[0] * value.shape[1], value.shape[2])
    square = value * value
    mine = jnp.concatenate([lanes(square[:, :split]), lanes(square[:, split:])], axis=0)
    squares[...] = jnp.broadcast_to(mine, squares.shape)


def total(terms):
    shape = terms[0].shape
    return pl.pallas_call(
        total_kernel,
        out_shape=[jax.ShapeDtypeStruct((4, *shape[1:]), F32)] * 2,
        compiler_params=params(10),
        cost_estimate=cost(0.5),
        name="total",
    )(*terms)


def total_squares(terms, split):
    return pl.pallas_call(
        functools.partial(squares_kernel, split),
        out_shape=[
            jax.ShapeDtypeStruct((8, *terms[0].shape[1:]), F32),
            jax.ShapeDtypeStruct((8, 2, 128), F32),
        ],
        compiler_params=params(10),
        cost_estimate=cost(0.5),
        name="total_squares",
    )(*terms)


def moments_kernel(qmean, qvar, omean, ovar, out):
    _, _, x, core = here()
    for part in range(2):
        index = place_of(first(x, core), part, core)
        start = 0
        for source in ((qmean, qvar), (omean, ovar)):
            width = source[0].shape[1] // RING
            at = pl.ds(pl.multiple_of(index * width, 128), width)
            for which in range(2):
                out[which, part, :, start : start + width] = source[which][:, at]
            start += width


def moments(qmean, qvar, omean, ovar):
    wide = (qmean.shape[1] + omean.shape[1]) // RING
    return pl.pallas_call(
        moments_kernel,
        out_shape=jax.ShapeDtypeStruct((2, 2, qmean.shape[0], wide), F32),
        compiler_params=params(4),
        cost_estimate=cost(1),
        name="moments",
    )(qmean, qvar, omean, ovar)


def direction_kernel(split, counts, mine, other, proj, *refs):
    moved, out = refs[:4], refs[4]
    z, y, _, core = here()
    own = second(y, core) * 2 + second(z, core)
    sums = jnp.sum(mine[...], axis=0) + jnp.sum(other[...], axis=0)
    sums = jnp.sum(sums, axis=1, keepdims=True)
    scales = [1.0 / jnp.maximum(jnp.sqrt(sums[k : k + 1] / counts[k]), 1.0) for k in range(2)]
    for offset in range(4):
        for part in range(2):
            shard = part * 4 + (own ^ offset)
            for k, at in enumerate((slice(0, split), slice(split, None))):
                scaled = scales[k] * proj[shard, :, at]
                new_mean = 0.8 * moved[offset][0, part, :, at] + 0.2 * scaled
                new_var = 0.9 * moved[offset][1, part, :, at] + 0.1 * scaled * scaled
                out[shard, :, at] = new_mean / jnp.sqrt(new_var)


def direction(mine, other, proj, moved, split, counts):
    return pl.pallas_call(
        functools.partial(direction_kernel, split, counts),
        out_shape=jax.ShapeDtypeStruct(proj.shape, F32),
        compiler_params=params(6),
        cost_estimate=cost(1.5),
        name="direction",
    )(mine, other, proj, *moved)


def late_kernel(rows, split, aliased, *refs):
    dirs, (qbasis, obasis, qweight, oweight) = refs[:4], refs[4:8]
    outs, scratch = refs[8 + aliased : 12 + aliased], refs[12 + aliased :]
    qstep, ostep, qcopy, ocopy = outs
    for spot in range(4):
        for pair in range(4):
            at = pl.ds(pl.multiple_of(rows_of(spot, pair) * rows, rows), rows)
            for ref, value in zip(scratch, halves(dirs[spot][pair])):
                ref[at, :] = value
    wide = scratch[0].shape[1]
    for basis, at, weight, step, copy in (
        (qbasis, slice(0, split), qweight, qstep, qcopy),
        (obasis, slice(split, wide), oweight, ostep, ocopy),
    ):
        value = jnp.dot(basis[...], scratch[0][:, at], preferred_element_type=F32)
        value += jnp.dot(basis[...], scratch[1][:, at], preferred_element_type=F32)
        step[...] = value
        copy[...] = (weight[...] - 0.05 * value).astype(BF16)


def late(dirs, qbasis, obasis, qweight, oweight, split, flip, before=()):
    _, rows, wide = dirs[0].shape
    rank = qbasis.shape[1]
    index = part_of(flip)
    qspec = pl.BlockSpec((qweight.shape[0], split), lambda i: (0, index(i)))
    ospec = pl.BlockSpec((oweight.shape[0], wide - split), lambda i: (0, index(i)))
    return pl.pallas_call(
        functools.partial(late_kernel, rows, split, len(before)),
        grid=(2,),
        in_specs=[pl.BlockSpec((4, rows, wide), lambda i: (i, 0, 0))] * 4
        + [
            pl.BlockSpec((qweight.shape[0], rank), lambda i: (lax.axis_index("fs"), 0)),
            pl.BlockSpec((oweight.shape[0], rank), lambda i: (lax.axis_index("fs"), 0)),
            qspec,
            ospec,
        ]
        + [pl.BlockSpec(memory_space=pl.ANY)] * len(before),
        out_specs=[qspec, ospec, qspec, ospec],
        out_shape=[
            jax.ShapeDtypeStruct(qweight.shape, F32),
            jax.ShapeDtypeStruct(oweight.shape, F32),
            jax.ShapeDtypeStruct(qweight.shape, BF16),
            jax.ShapeDtypeStruct(oweight.shape, BF16),
        ],
        scratch_shapes=[pltpu.VMEM((rank, wide), BF16)] * 2,
        input_output_aliases={8 + k: k for k in range(len(before))},
        compiler_params=params(12),
        cost_estimate=cost(2),
    )(*dirs, qbasis, obasis, qweight, oweight, *before)


def swap(value, phase, offset):
    return lax.ppermute(value, AXES, partners(phase, offset))


def on_device(
    saved_latent,
    query_cotangent,
    mix_cotangent,
    head_outputs,
    query_weight,
    out_weight,
    query_basis,
    out_basis,
    query_mean,
    query_var,
    out_mean,
    out_var,
):
    rank, cores = query_basis.shape[1], lax.axis_size("tp")
    split = query_cotangent.shape[1] // RING
    counts = (
        float(rank * query_cotangent.shape[1] * cores),
        float(rank * head_outputs.shape[1] * cores),
    )
    qlow, olow, *far = front(
        saved_latent, mix_cotangent, query_basis, out_basis, query_cotangent, head_outputs
    )
    near = near_blocks(qlow, olow, query_cotangent, head_outputs)
    held = moments(query_mean, query_var, out_mean, out_var)
    came = {}
    for k in (3, 2, 1, 0):
        came[4 + k] = swap(far[k], 1, 4 + k)
    came |= {k: swap(near[k], 1, k) for k in (3, 2, 1)}
    moved = [swap(held, 2, k) for k in (1, 2, 3)]
    near, came, moved = lax.optimization_barrier((near, came, moved))
    moved = [held] + moved
    chains = list(total([near[0]] + [came[k] for k in range(1, 8)]))
    for step in range(3):
        others = [swap(v, 2, order[step]) for v, order in zip(chains, ORDERS)]
        if step < 2:
            chains = [v + w for v, w in zip(chains, others)]
    last = [v for pair in zip(chains, others) for v in pair]
    proj, squares = total_squares(last, split)
    mine = lax.all_to_all(squares, AXES, 0, 0, tiled=True, axis_index_groups=first_groups())
    other = lax.ppermute(mine, "tp", [(0, 1), (1, 0)])
    dirs = direction(mine, other, proj, moved, split, counts)
    spread = [dirs] + [swap(dirs, 1, k) for k in range(1, 8)]
    steps = late(spread[:4], query_basis, out_basis, query_weight, out_weight, split, 0)
    return tuple(late(spread[4:], query_basis, out_basis, query_weight, out_weight, split, 1, steps))


def solution(mesh):
    placed = (
        P(("fs", "rep"), None),
        P(("fs", "rep"), "tp"),
        P(("fs", "rep"), None),
        P(("fs", "rep"), "tp"),
        P("fs", "tp"),
        P("fs", "tp"),
        P(),
        P(),
        P("fs", "tp"),
        P("fs", "tp"),
        P("fs", "tp"),
        P("fs", "tp"),
    )
    return jax.shard_map(
        on_device,
        mesh=mesh,
        in_specs=placed,
        out_specs=(P("fs", "tp"), P("fs", "tp"), P("fs", "tp"), P("fs", "tp")),
        check_vma=False,
    )
```

profile of v0, /device:TPU:1, one launch (start us, length us, event | category | flops | bytes accessed | tf_op | source)
XLA Modules:
  0.0 107.8 jit_solution(8125748940294486067)
XLA Ops:
  0.7 9.4 %front.1 = (bf16[2,256,768]{2,1,0:T(8,128)(2,1)S(1)}, bf16[2,256,768]{2,1,0:T(8,128)(2,1)S(1)}, f32[8,16,640]{2,1,0:T(8,128)S(1)}, f32[8,16,640]{2,1,0:T(8,128)S...) custom-call(bf16[768,2048]{1,0:T(8,128)(2,1)} %latent.1, bf16[768,4096]{1,0:T(8,128)(2,1)} %mix.1, ...), custom_call_target="tpu_custom_call" | custom-call | flops 700000000 | bytes 7000000 | tf_op jit(solution)/shard_map/front/pallas_call | solution.py:194
  11.6 4.7 %collective-permute-start = (f32[8,16,640]{2,1,0:T(8,128)S(1)}, f32[8,16,640]{2,1,0:T(8,128)S(1)}, u32[]{:S(2)}, u32[]{:S(2)}) collective-permute-start(f32[8,16,640]{2,1,0:T(8,128)S(1)} %get-tuple-element.36), channel_id=1, source_target_pairs={{0,32},{1,97},{2,34},{3,99},{4,36},{5,101},{6,38},{7,103},{8,40},{... | collective-permute-start | bytes 983048 | tf_op jit(solution)/shard_map/ppermute | solution.py:383
  16.3 2.8 %collective-permute-start.1 = (f32[8,16,640]{2,1,0:T(8,128)S(1)}, f32[8,16,640]{2,1,0:T(8,128)S(1)}, u32[]{:S(2)}, u32[]{:S(2)}) collective-permute-start(f32[8,16,640]{2,1,0:T(8,128)S(1)} %get-tuple-element.37), channel_id=1, source_target_pairs={{0,8},{1,25},{2,10},{3,27},{4,12},{5,29},{6,14},{7,31},{8,0},{9,17... | collective-permute-start | bytes 983048 | tf_op jit(solution)/shard_map/ppermute | solution.py:383
  19.9 1.9 %collective-permute-start.7 = (f32[2,2,16,640]{3,2,1,0:T(8,128)S(1)}, f32[2,2,16,640]{3,2,1,0:T(8,128)S(1)}, u32[]{:S(2)}, u32[]{:S(2)}) collective-permute-start(f32[2,2,16,640]{3,2,1,0:T(8,128)S(1)} %moments.1.refs_0_), channel_id=1, source_target_pairs={{0,96},{1,33},{2,98},{3,35},{4,100},{5,37},{6,102},{7,39},{8,104},... | collective-permute-start | bytes 491528 | tf_op jit(solution)/shard_map/ppermute | solution.py:383
  21.8 2.7 %collective-permute-done.9.refs_3_ = f32[2,2,16,640]{3,2,1,0:T(8,128)S(1)} collective-permute-done((f32[2,2,16,640]{3,2,1,0:T(8,128)S(1)}, f32[2,2,16,640]{3,2,1,0:T(8,128)S(1)}, u32[]{:S(2)}, u32[]{:S(2)}) %collective-permute-start.9) | collective-permute-done | bytes 163872 | tf_op jit(solution)/shard_map/ppermute | solution.py:383
  25.3 2.5 %collective-permute-start.3 = (f32[8,16,640]{2,1,0:T(8,128)S(1)}, f32[8,16,640]{2,1,0:T(8,128)S(1)}, u32[]{:S(2)}, u32[]{:S(2)}) collective-permute-start(f32[8,16,640]{2,1,0:T(8,128)S(1)} %get-tuple-element.39), channel_id=1, source_target_pairs={{0,2},{1,7},{2,0},{3,5},{4,6},{5,3},{6,4},{7,1},{8,10},{9,15},{10,... | collective-permute-start | bytes 983048 | tf_op jit(solution)/shard_map/ppermute | solution.py:383
  27.8 2.8 %collective-permute-start.4 = (f32[8,16,640]{2,1,0:T(8,128)S(1)}, f32[8,16,640]{2,1,0:T(8,128)S(1)}, u32[]{:S(2)}, u32[]{:S(2)}) collective-permute-start(f32[8,16,640]{2,1,0:T(8,128)S(1)} %get-tuple-element.40), channel_id=1, source_target_pairs={{0,34},{1,103},{2,32},{3,101},{4,38},{5,99},{6,36},{7,97},{8,42},{... | collective-permute-start | bytes 983048 | tf_op jit(solution)/shard_map/ppermute | solution.py:383
  30.6 3.6 %collective-permute-start.5 = (f32[8,16,640]{2,1,0:T(8,128)S(1)}, f32[8,16,640]{2,1,0:T(8,128)S(1)}, u32[]{:S(2)}, u32[]{:S(2)}) collective-permute-start(f32[8,16,640]{2,1,0:T(8,128)S(1)} %get-tuple-element.41), channel_id=1, source_target_pairs={{0,10},{1,31},{2,8},{3,29},{4,14},{5,27},{6,12},{7,25},{8,2},{9,23... | collective-permute-start | bytes 983048 | tf_op jit(solution)/shard_map/ppermute | solution.py:383
  35.9 2.7 %collective-permute-done.4.refs_5_ = f32[8,16,640]{2,1,0:T(8,128)S(1)} collective-permute-done((f32[8,16,640]{2,1,0:T(8,128)S(1)}, f32[8,16,640]{2,1,0:T(8,128)S(1)}, u32[]{:S(2)}, u32[]{:S(2)}) %collective-permute-start.4) | collective-permute-done | bytes 327712 | tf_op jit(solution)/shard_map/ppermute | solution.py:383
  38.6 4.1 %collective-permute-done.5.refs_6_ = f32[8,16,640]{2,1,0:T(8,128)S(1)} collective-permute-done((f32[8,16,640]{2,1,0:T(8,128)S(1)}, f32[8,16,640]{2,1,0:T(8,128)S(1)}, u32[]{:S(2)}, u32[]{:S(2)}) %collective-permute-start.5) | collective-permute-done | bytes 327712 | tf_op jit(solution)/shard_map/ppermute | solution.py:383
  42.7 4.6 %collective-permute-done.6.refs_7_ = f32[8,16,640]{2,1,0:T(8,128)S(1)} collective-permute-done((f32[8,16,640]{2,1,0:T(8,128)S(1)}, f32[8,16,640]{2,1,0:T(8,128)S(1)}, u32[]{:S(2)}, u32[]{:S(2)}) %collective-permute-start.6) | collective-permute-done | bytes 327712 | tf_op jit(solution)/shard_map/ppermute | solution.py:383
  47.6 4.4 %collective-permute-done.10 = f32[4,16,640]{2,1,0:T(8,128)S(1)} collective-permute-done((f32[4,16,640]{2,1,0:T(8,128)S(1)}, f32[4,16,640]{2,1,0:T(8,128)S(1)}, u32[]{:S(2)}, u32[]{:S(2)}) %collective-permute-start.10) | collective-permute-done | bytes 163872 | tf_op jit(solution)/shard_map/ppermute | solution.py:383
  52.2 4.0 %collective-permute-done.11 = f32[4,16,640]{2,1,0:T(8,128)S(1)} collective-permute-done((f32[4,16,640]{2,1,0:T(8,128)S(1)}, f32[4,16,640]{2,1,0:T(8,128)S(1)}, u32[]{:S(2)}, u32[]{:S(2)}) %collective-permute-start.11) | collective-permute-done | bytes 163872 | tf_op jit(solution)/shard_map/ppermute | solution.py:383
  58.1 2.7 %collective-permute-done.12.refs_1_ = f32[4,16,640]{2,1,0:T(8,128)S(1)} collective-permute-done((f32[4,16,640]{2,1,0:T(8,128)S(1)}, f32[4,16,640]{2,1,0:T(8,128)S(1)}, u32[]{:S(2)}, u32[]{:S(2)}) %collective-permute-start.12) | collective-permute-done | bytes 163872 | tf_op jit(solution)/shard_map/ppermute | solution.py:383
  61.2 12.3 %all_to_all.5.mine = f32[8,2,128]{2,1,0:T(2,128)S(1)} all-to-all(f32[8,2,128]{2,1,0:T(2,128)S(1)} %get-tuple-element.53), channel_id=1, replica_groups={{0,32,8,40,2,34,10,42},{1,97,25,121,7,103,31,127},{3,99,27,123,5,101,29..., dimensions={0} | all-to-all | bytes 16384 | tf_op jit(solution)/shard_map/all_to_all | solution.py:425
  73.5 3.7 %collective-permute-start.16 = (f32[8,2,128]{2,1,0:T(2,128)S(1)}, f32[8,2,128]{2,1,0:T(2,128)S(1)}, u32[]{:S(2)}, u32[]{:S(2)}) collective-permute-start(f32[8,2,128]{2,1,0:T(2,128)S(1)} %all_to_all.5.mine), channel_id=1, source_target_pairs={{0,1},{1,0},{2,3},{3,2},{4,5},{5,4},{6,7},{7,6},{8,9},{9,8},{10,11... | collective-permute-start | bytes 24584 | tf_op jit(solution)/shard_map/ppermute | solution.py:426
  78.3 5.2 %collective-permute-start.23 = (f32[8,16,640]{2,1,0:T(8,128)S(1)}, f32[8,16,640]{2,1,0:T(8,128)S(1)}, u32[]{:S(2)}, u32[]{:S(2)}) collective-permute-start(f32[8,16,640]{2,1,0:T(8,128)S(1)} %direction.1.refs_0_), channel_id=1, source_target_pairs={{0,40},{1,121},{2,42},{3,123},{4,44},{5,125},{6,46},{7,127},{8,32}... | collective-permute-start | bytes 983048 | tf_op jit(solution)/shard_map/ppermute | solution.py:383
  83.9 4.5 %collective-permute-start.20 = (f32[8,16,640]{2,1,0:T(8,128)S(1)}, f32[8,16,640]{2,1,0:T(8,128)S(1)}, u32[]{:S(2)}, u32[]{:S(2)}) collective-permute-start(f32[8,16,640]{2,1,0:T(8,128)S(1)} %direction.1.refs_0_), channel_id=1, source_target_pairs={{0,42},{1,127},{2,40},{3,125},{4,46},{5,123},{6,44},{7,121},{8,34}... | collective-permute-start | bytes 983048 | tf_op jit(solution)/shard_map/ppermute | solution.py:383
  88.4 2.3 %collective-permute-start.19 = (f32[8,16,640]{2,1,0:T(8,128)S(1)}, f32[8,16,640]{2,1,0:T(8,128)S(1)}, u32[]{:S(2)}, u32[]{:S(2)}) collective-permute-start(f32[8,16,640]{2,1,0:T(8,128)S(1)} %direction.1.refs_0_), channel_id=1, source_target_pairs={{0,10},{1,31},{2,8},{3,29},{4,14},{5,27},{6,12},{7,25},{8,2},{9,23... | collective-permute-start | bytes 983048 | tf_op jit(solution)/shard_map/ppermute | solution.py:383
  90.7 2.5 %collective-permute-start.18 = (f32[8,16,640]{2,1,0:T(8,128)S(1)}, f32[8,16,640]{2,1,0:T(8,128)S(1)}, u32[]{:S(2)}, u32[]{:S(2)}) collective-permute-start(f32[8,16,640]{2,1,0:T(8,128)S(1)} %direction.1.refs_0_), channel_id=1, source_target_pairs={{0,34},{1,103},{2,32},{3,101},{4,38},{5,99},{6,36},{7,97},{8,42},{... | collective-permute-start | bytes 983048 | tf_op jit(solution)/shard_map/ppermute | solution.py:383
  94.5 2.0 %shard_map.147 = (f32[128,1536]{1,0:T(8,128)}, f32[256,1024]{1,0:T(8,128)}, bf16[128,1536]{1,0:T(8,128)(2,1)}, bf16[256,1024]{1,0:T(8,128)(2,1)}) custom-call(f32[8,16,640]{2,1,0:T(8,128)S(1)} %direction.1.refs_0_, f32[8,16,640]{2,1,0:T(8,128)S(1)} %collective-permute-done.21.refs_1_, f32[8,16,640]{2,1,0:T(8,128)S(1)} %collective-permute-done.22.refs_2_, ...), custom_call_target="tpu_custom_call" | custom-call | flops 200000000 | bytes 2000000 | tf_op jit(solution)/shard_map/pallas_call | solution.py:357
  96.4 2.2 %collective-permute-done.19.refs_2_ = f32[8,16,640]{2,1,0:T(8,128)S(1)} collective-permute-done((f32[8,16,640]{2,1,0:T(8,128)S(1)}, f32[8,16,640]{2,1,0:T(8,128)S(1)}, u32[]{:S(2)}, u32[]{:S(2)}) %collective-permute-start.19) | collective-permute-done | bytes 327712 | tf_op jit(solution)/shard_map/ppermute | solution.py:383
  98.7 3.5 %collective-permute-done.18.refs_1_ = f32[8,16,640]{2,1,0:T(8,128)S(1)} collective-permute-done((f32[8,16,640]{2,1,0:T(8,128)S(1)}, f32[8,16,640]{2,1,0:T(8,128)S(1)}, u32[]{:S(2)}, u32[]{:S(2)}) %collective-permute-start.18) | collective-permute-done | bytes 327712 | tf_op jit(solution)/shard_map/ppermute | solution.py:383
  102.2 3.8 %collective-permute-done.17.refs_0_ = f32[8,16,640]{2,1,0:T(8,128)S(1)} collective-permute-done((f32[8,16,640]{2,1,0:T(8,128)S(1)}, f32[8,16,640]{2,1,0:T(8,128)S(1)}, u32[]{:S(2)}, u32[]{:S(2)}) %collective-permute-start.17) | collective-permute-done | bytes 327712 | tf_op jit(solution)/shard_map/ppermute | solution.py:383
  (57 shorter events, 12.1 us)
Async XLA Ops:
  11.6 19.0 %collective-permute-start = (f32[8,16,640]{2,1,0:T(8,128)S(1)}, f32[8,16,640]{2,1,0:T(8,128)S(1)}, u32[]{:S(2)}, u32[]{:S(2)}) collective-permute-start(f32[8,16,640]{2,1,0:T(8,128)S(1)} %get-tuple-element.36), channel_id=1, source_target_pairs={{0,32},{1,97},{2,34},{3,99},{4,36},{5,101},{6,38},{7,103},{8,40},{... | collective-permute-start | bytes 983048 | tf_op jit(solution)/shard_map/ppermute | solution.py:383
  16.3 18.0 %collective-permute-start.1 = (f32[8,16,640]{2,1,0:T(8,128)S(1)}, f32[8,16,640]{2,1,0:T(8,128)S(1)}, u32[]{:S(2)}, u32[]{:S(2)}) collective-permute-start(f32[8,16,640]{2,1,0:T(8,128)S(1)} %get-tuple-element.37), channel_id=1, source_target_pairs={{0,8},{1,25},{2,10},{3,27},{4,12},{5,29},{6,14},{7,31},{8,0},{9,17... | collective-permute-start | bytes 983048 | tf_op jit(solution)/shard_map/ppermute | solution.py:383
  19.1 5.4 %collective-permute-start.9 = (f32[2,2,16,640]{3,2,1,0:T(8,128)S(1)}, f32[2,2,16,640]{3,2,1,0:T(8,128)S(1)}, u32[]{:S(2)}, u32[]{:S(2)}) collective-permute-start(f32[2,2,16,640]{3,2,1,0:T(8,128)S(1)} %moments.1.refs_0_), channel_id=1, source_target_pairs={{0,120},{1,41},{2,122},{3,43},{4,124},{5,45},{6,126},{7,47},{8,112... | collective-permute-start | bytes 491528 | tf_op jit(solution)/shard_map/ppermute | solution.py:383
  19.2 6.1 %collective-permute-start.8 = (f32[2,2,16,640]{3,2,1,0:T(8,128)S(1)}, f32[2,2,16,640]{3,2,1,0:T(8,128)S(1)}, u32[]{:S(2)}, u32[]{:S(2)}) collective-permute-start(f32[2,2,16,640]{3,2,1,0:T(8,128)S(1)} %moments.1.refs_0_), channel_id=1, source_target_pairs={{0,24},{1,9},{2,26},{3,11},{4,28},{5,13},{6,30},{7,15},{8,16},{9,1... | collective-permute-start | bytes 491528 | tf_op jit(solution)/shard_map/ppermute | solution.py:383
  19.9 7.9 %collective-permute-start.7 = (f32[2,2,16,640]{3,2,1,0:T(8,128)S(1)}, f32[2,2,16,640]{3,2,1,0:T(8,128)S(1)}, u32[]{:S(2)}, u32[]{:S(2)}) collective-permute-start(f32[2,2,16,640]{3,2,1,0:T(8,128)S(1)} %moments.1.refs_0_), channel_id=1, source_target_pairs={{0,96},{1,33},{2,98},{3,35},{4,100},{5,37},{6,102},{7,39},{8,104},... | collective-permute-start | bytes 491528 | tf_op jit(solution)/shard_map/ppermute | solution.py:383
  24.5 11.4 %collective-permute-start.2 = (f32[8,16,640]{2,1,0:T(8,128)S(1)}, f32[8,16,640]{2,1,0:T(8,128)S(1)}, u32[]{:S(2)}, u32[]{:S(2)}) collective-permute-start(f32[8,16,640]{2,1,0:T(8,128)S(1)} %get-tuple-element.38), channel_id=1, source_target_pairs={{0,40},{1,121},{2,42},{3,123},{4,44},{5,125},{6,46},{7,127},{8,32}... | collective-permute-start | bytes 983048 | tf_op jit(solution)/shard_map/ppermute | solution.py:383
  25.3 10.6 %collective-permute-start.3 = (f32[8,16,640]{2,1,0:T(8,128)S(1)}, f32[8,16,640]{2,1,0:T(8,128)S(1)}, u32[]{:S(2)}, u32[]{:S(2)}) collective-permute-start(f32[8,16,640]{2,1,0:T(8,128)S(1)} %get-tuple-element.39), channel_id=1, source_target_pairs={{0,2},{1,7},{2,0},{3,5},{4,6},{5,3},{6,4},{7,1},{8,10},{9,15},{10,... | collective-permute-start | bytes 983048 | tf_op jit(solution)/shard_map/ppermute | solution.py:383
  27.8 10.8 %collective-permute-start.4 = (f32[8,16,640]{2,1,0:T(8,128)S(1)}, f32[8,16,640]{2,1,0:T(8,128)S(1)}, u32[]{:S(2)}, u32[]{:S(2)}) collective-permute-start(f32[8,16,640]{2,1,0:T(8,128)S(1)} %get-tuple-element.40), channel_id=1, source_target_pairs={{0,34},{1,103},{2,32},{3,101},{4,38},{5,99},{6,36},{7,97},{8,42},{... | collective-permute-start | bytes 983048 | tf_op jit(solution)/shard_map/ppermute | solution.py:383
  30.6 12.0 %collective-permute-start.5 = (f32[8,16,640]{2,1,0:T(8,128)S(1)}, f32[8,16,640]{2,1,0:T(8,128)S(1)}, u32[]{:S(2)}, u32[]{:S(2)}) collective-permute-start(f32[8,16,640]{2,1,0:T(8,128)S(1)} %get-tuple-element.41), channel_id=1, source_target_pairs={{0,10},{1,31},{2,8},{3,29},{4,14},{5,27},{6,12},{7,25},{8,2},{9,23... | collective-permute-start | bytes 983048 | tf_op jit(solution)/shard_map/ppermute | solution.py:383
  34.2 13.0 %collective-permute-start.6 = (f32[8,16,640]{2,1,0:T(8,128)S(1)}, f32[8,16,640]{2,1,0:T(8,128)S(1)}, u32[]{:S(2)}, u32[]{:S(2)}) collective-permute-start(f32[8,16,640]{2,1,0:T(8,128)S(1)} %get-tuple-element.42), channel_id=1, source_target_pairs={{0,42},{1,127},{2,40},{3,125},{4,46},{5,123},{6,44},{7,121},{8,34}... | collective-permute-start | bytes 983048 | tf_op jit(solution)/shard_map/ppermute | solution.py:383
  47.4 4.5 %collective-permute-start.10 = (f32[4,16,640]{2,1,0:T(8,128)S(1)}, f32[4,16,640]{2,1,0:T(8,128)S(1)}, u32[]{:S(2)}, u32[]{:S(2)}) collective-permute-start(f32[4,16,640]{2,1,0:T(8,128)S(1)} %get-tuple-element.51), channel_id=1, source_target_pairs={{0,6},{1,3},{2,4},{3,1},{4,2},{5,7},{6,0},{7,5},{8,14},{9,11},{10,... | collective-permute-start | bytes 491528 | tf_op jit(solution)/shard_map/ppermute | solution.py:383
  47.5 4.6 %collective-permute-start.13 = (f32[4,16,640]{2,1,0:T(8,128)S(1)}, f32[4,16,640]{2,1,0:T(8,128)S(1)}, u32[]{:S(2)}, u32[]{:S(2)}) collective-permute-start(f32[4,16,640]{2,1,0:T(8,128)S(1)} %get-tuple-element.52), channel_id=1, source_target_pairs={{0,24},{1,9},{2,26},{3,11},{4,28},{5,13},{6,30},{7,15},{8,16},{9,1... | collective-permute-start | bytes 491528 | tf_op jit(solution)/shard_map/ppermute | solution.py:383
  52.0 4.2 %collective-permute-start.11 = (f32[4,16,640]{2,1,0:T(8,128)S(1)}, f32[4,16,640]{2,1,0:T(8,128)S(1)}, u32[]{:S(2)}, u32[]{:S(2)}) collective-permute-start(f32[4,16,640]{2,1,0:T(8,128)S(1)} %add.12), channel_id=1, source_target_pairs={{0,24},{1,9},{2,26},{3,11},{4,28},{5,13},{6,30},{7,15},{8,16},{9,1... | collective-permute-start | bytes 491528 | tf_op jit(solution)/shard_map/ppermute | solution.py:383
  52.1 4.2 %collective-permute-start.14 = (f32[4,16,640]{2,1,0:T(8,128)S(1)}, f32[4,16,640]{2,1,0:T(8,128)S(1)}, u32[]{:S(2)}, u32[]{:S(2)}) collective-permute-start(f32[4,16,640]{2,1,0:T(8,128)S(1)} %add.14), channel_id=1, source_target_pairs={{0,96},{1,33},{2,98},{3,35},{4,100},{5,37},{6,102},{7,39},{8,104},... | collective-permute-start | bytes 491528 | tf_op jit(solution)/shard_map/ppermute | solution.py:383
  56.3 4.5 %collective-permute-start.12 = (f32[4,16,640]{2,1,0:T(8,128)S(1)}, f32[4,16,640]{2,1,0:T(8,128)S(1)}, u32[]{:S(2)}, u32[]{:S(2)}) collective-permute-start(f32[4,16,640]{2,1,0:T(8,128)S(1)} %add.13.refs_0_), channel_id=1, source_target_pairs={{0,96},{1,33},{2,98},{3,35},{4,100},{5,37},{6,102},{7,39},{8,104},... | collective-permute-start | bytes 491528 | tf_op jit(solution)/shard_map/ppermute | solution.py:383
  56.4 4.7 %collective-permute-start.15 = (f32[4,16,640]{2,1,0:T(8,128)S(1)}, f32[4,16,640]{2,1,0:T(8,128)S(1)}, u32[]{:S(2)}, u32[]{:S(2)}) collective-permute-start(f32[4,16,640]{2,1,0:T(8,128)S(1)} %add.15.refs_2_), channel_id=1, source_target_pairs={{0,6},{1,3},{2,4},{3,1},{4,2},{5,7},{6,0},{7,5},{8,14},{9,11},{10,... | collective-permute-start | bytes 491528 | tf_op jit(solution)/shard_map/ppermute | solution.py:383
  73.5 4.6 %collective-permute-start.16 = (f32[8,2,128]{2,1,0:T(2,128)S(1)}, f32[8,2,128]{2,1,0:T(2,128)S(1)}, u32[]{:S(2)}, u32[]{:S(2)}) collective-permute-start(f32[8,2,128]{2,1,0:T(2,128)S(1)} %all_to_all.5.mine), channel_id=1, source_target_pairs={{0,1},{1,0},{2,3},{3,2},{4,5},{5,4},{6,7},{7,6},{8,9},{9,8},{10,11... | collective-permute-start | bytes 24584 | tf_op jit(solution)/shard_map/ppermute | solution.py:426
  78.3 12.4 %collective-permute-start.23 = (f32[8,16,640]{2,1,0:T(8,128)S(1)}, f32[8,16,640]{2,1,0:T(8,128)S(1)}, u32[]{:S(2)}, u32[]{:S(2)}) collective-permute-start(f32[8,16,640]{2,1,0:T(8,128)S(1)} %direction.1.refs_0_), channel_id=1, source_target_pairs={{0,40},{1,121},{2,42},{3,123},{4,44},{5,125},{6,46},{7,127},{8,32}... | collective-permute-start | bytes 983048 | tf_op jit(solution)/shard_map/ppermute | solution.py:383
  83.5 9.7 %collective-permute-start.22 = (f32[8,16,640]{2,1,0:T(8,128)S(1)}, f32[8,16,640]{2,1,0:T(8,128)S(1)}, u32[]{:S(2)}, u32[]{:S(2)}) collective-permute-start(f32[8,16,640]{2,1,0:T(8,128)S(1)} %direction.1.refs_0_), channel_id=1, source_target_pairs={{0,8},{1,25},{2,10},{3,27},{4,12},{5,29},{6,14},{7,31},{8,0},{9,17... | collective-permute-start | bytes 983048 | tf_op jit(solution)/shard_map/ppermute | solution.py:383
  83.5 10.9 %collective-permute-start.21 = (f32[8,16,640]{2,1,0:T(8,128)S(1)}, f32[8,16,640]{2,1,0:T(8,128)S(1)}, u32[]{:S(2)}, u32[]{:S(2)}) collective-permute-start(f32[8,16,640]{2,1,0:T(8,128)S(1)} %direction.1.refs_0_), channel_id=1, source_target_pairs={{0,32},{1,97},{2,34},{3,99},{4,36},{5,101},{6,38},{7,103},{8,40},{... | collective-permute-start | bytes 983048 | tf_op jit(solution)/shard_map/ppermute | solution.py:383
  83.9 12.6 %collective-permute-start.20 = (f32[8,16,640]{2,1,0:T(8,128)S(1)}, f32[8,16,640]{2,1,0:T(8,128)S(1)}, u32[]{:S(2)}, u32[]{:S(2)}) collective-permute-start(f32[8,16,640]{2,1,0:T(8,128)S(1)} %direction.1.refs_0_), channel_id=1, source_target_pairs={{0,42},{1,127},{2,40},{3,125},{4,46},{5,123},{6,44},{7,121},{8,34}... | collective-permute-start | bytes 983048 | tf_op jit(solution)/shard_map/ppermute | solution.py:383
  88.4 10.3 %collective-permute-start.19 = (f32[8,16,640]{2,1,0:T(8,128)S(1)}, f32[8,16,640]{2,1,0:T(8,128)S(1)}, u32[]{:S(2)}, u32[]{:S(2)}) collective-permute-start(f32[8,16,640]{2,1,0:T(8,128)S(1)} %direction.1.refs_0_), channel_id=1, source_target_pairs={{0,10},{1,31},{2,8},{3,29},{4,14},{5,27},{6,12},{7,25},{8,2},{9,23... | collective-permute-start | bytes 983048 | tf_op jit(solution)/shard_map/ppermute | solution.py:383
  90.7 11.5 %collective-permute-start.18 = (f32[8,16,640]{2,1,0:T(8,128)S(1)}, f32[8,16,640]{2,1,0:T(8,128)S(1)}, u32[]{:S(2)}, u32[]{:S(2)}) collective-permute-start(f32[8,16,640]{2,1,0:T(8,128)S(1)} %direction.1.refs_0_), channel_id=1, source_target_pairs={{0,34},{1,103},{2,32},{3,101},{4,38},{5,99},{6,36},{7,97},{8,42},{... | collective-permute-start | bytes 983048 | tf_op jit(solution)/shard_map/ppermute | solution.py:383
  93.2 12.8 %collective-permute-start.17 = (f32[8,16,640]{2,1,0:T(8,128)S(1)}, f32[8,16,640]{2,1,0:T(8,128)S(1)}, u32[]{:S(2)}, u32[]{:S(2)}) collective-permute-start(f32[8,16,640]{2,1,0:T(8,128)S(1)} %direction.1.refs_0_), channel_id=1, source_target_pairs={{0,2},{1,7},{2,0},{3,5},{4,6},{5,3},{6,4},{7,1},{8,10},{9,15},{10,... | collective-permute-start | bytes 983048 | tf_op jit(solution)/shard_map/ppermute | solution.py:383
  (10 other events, 242.9 us)
where the time goes:
time: 108 us
  starting transfers between devices  42.7 us (40%)
  waiting for transfers between devices  36.6 us (34%)
  Pallas kernels  15.2 us (14%)
  blocking collectives  12.3 us (11%)
    ppermute x23, starting transfers between devices, swap(): return lax.ppermute(value, AXES, partners(phase, offset))  38.9 us
    ppermute x23, waiting for transfers between devices, swap(): return lax.ppermute(value, AXES, partners(phase, offset))  35.8 us
    all_to_all x1, blocking collectives, on_device(): lax.all_to_all(squares, AXES, 0, 0, tiled=True, axis_index_groups=first_g...  12.3 us
    pallas_call x1, Pallas kernels, front(): pl.pallas_call(functools.partial(front_kernel, rows), in_specs=[pl.BlockS...  9.43 us
    pallas_call x2, Pallas kernels, late(): pl.pallas_call(functools.partial(late_kernel, rows, split, len(before)),...  3.83 us
    ppermute x1, starting transfers between devices, on_device(): other = lax.ppermute(mine, 'tp', [(0, 1), (1, 0)])  3.74 us
  transfers between devices with their start and end apart: 24, of which 13 were waited for; matrix products, arithmetic and copies ran while one was open for 0% of the time, Pallas kernels for 2%

commit v1 on v0

--- a/solution.py
+++ b/solution.py
@@ -16,6 +16,8 @@
 FRONT = 51
 STEPS = 4
 AHEAD = 24
+GATHER = (7, 6, 1, 5, 2, 3, 4)
+SPREAD = (3, 1, 6, 2, 5, 7, 4)
 ORDERS = ((4, 2, 1), (2, 1, 4))
 
 
@@ -127,7 +129,7 @@
         waits.setdefault(key, []).append(len(copies))
         copies.append(pltpu.make_async_copy(source, target, sems.at[len(copies)]))
 
-    for name, tokens, basis, inside, beside in (("m", mix, obasis, ms, os), ("x", latent, qbasis, xs, qs)):
+    for name, tokens, basis, inside, beside in (("x", latent, qbasis, xs, qs), ("m", mix, obasis, ms, os)):
         wide = tokens.shape[1] // STEPS
         for k in range(STEPS):
             at = pl.ds(k * wide, wide)
@@ -153,7 +155,7 @@
 
     apart = lax.axis_index("fs") >= 0
     ahead(AHEAD)
-    for name, inside, beside, low in (("m", ms, os, olow), ("x", xs, qs, qlow)):
+    for name, inside, beside, low in (("x", xs, qs, qlow), ("m", ms, os, olow)):
         wide = inside.shape[1] // STEPS
         for k in range(STEPS):
 
@@ -409,15 +411,16 @@
     near = near_blocks(qlow, olow, query_cotangent, head_outputs)
     held = moments(query_mean, query_var, out_mean, out_var)
     came = {}
-    for k in (3, 2, 1, 0):
-        came[4 + k] = swap(far[k], 1, 4 + k)
-    came |= {k: swap(near[k], 1, k) for k in (3, 2, 1)}
-    moved = [swap(held, 2, k) for k in (1, 2, 3)]
-    near, came, moved = lax.optimization_barrier((near, came, moved))
-    moved = [held] + moved
+    for k in GATHER:
+        came[k] = swap(far[k - 4] if k > 3 else near[k], 1, k)
+    moved = [held]
+    for k in (1, 2, 3):
+        moved.append(swap(held, 2, k))
     chains = list(total([near[0]] + [came[k] for k in range(1, 8)]))
     for step in range(3):
-        others = [swap(v, 2, order[step]) for v, order in zip(chains, ORDERS)]
+        others = []
+        for v, order in zip(chains, ORDERS):
+            others.append(swap(v, 2, order[step]))
         if step < 2:
             chains = [v + w for v, w in zip(chains, others)]
     last = [v for pair in zip(chains, others) for v in pair]
@@ -425,7 +428,10 @@
     mine = lax.all_to_all(squares, AXES, 0, 0, tiled=True, axis_index_groups=first_groups())
     other = lax.ppermute(mine, "tp", [(0, 1), (1, 0)])
     dirs = direction(mine, other, proj, moved, split, counts)
-    spread = [dirs] + [swap(dirs, 1, k) for k in range(1, 8)]
+    spread = {0: dirs}
+    for k in SPREAD:
+        spread[k] = swap(dirs, 1, k)
+    spread = [spread[k] for k in range(8)]
     steps = late(spread[:4], query_basis, out_basis, query_weight, out_weight, split, 0)
     return tuple(late(spread[4:], query_basis, out_basis, query_weight, out_weight, split, 1, steps))
 

time: 108 us -> 99.5 us (0.921)
  the two profiles are of different devices: /device:TPU:1 before, /device:TPU:0 now
where the time goes in v1:
time: 99.5 us; the launch traced here: 98.1 us
  starting transfers between devices  43.1 us (43%)
  waiting for transfers between devices  30.7 us (31%)
  Pallas kernels  15.4 us (15%)
  blocking collectives  7.97 us (8%)
    ppermute x23, starting transfers between devices, swap(): return lax.ppermute(value, AXES, partners(phase, offset))  43.1 us
    ppermute x23, waiting for transfers between devices, swap(): return lax.ppermute(value, AXES, partners(phase, offset))  29.5 us
    pallas_call x1, Pallas kernels, front(): pl.pallas_call(functools.partial(front_kernel, rows), in_specs=[pl.BlockS...  9.57 us
    all_to_all x1, blocking collectives, on_device(): lax.all_to_all(squares, AXES, 0, 0, tiled=True, axis_index_groups=first_g...  7.97 us
    pallas_call x2, Pallas kernels, late(): pl.pallas_call(functools.partial(late_kernel, rows, split, len(before)),...  3.83 us
  transfers between devices with their start and end apart: 24, of which 11 were waited for; matrix products, arithmetic and copies ran while one was open for 0% of the time, Pallas kernels for 2%

profile of v1, /device:TPU:0, one launch (start us, length us, event | category | flops | bytes accessed | tf_op | source)
XLA Modules:
  0.0 98.1 jit_solution(13078091462462989348)
XLA Ops:
  0.7 9.6 %front.1 = (bf16[2,256,768]{2,1,0:T(8,128)(2,1)S(1)}, bf16[2,256,768]{2,1,0:T(8,128)(2,1)S(1)}, f32[8,16,640]{2,1,0:T(8,128)S(1)}, f32[8,16,640]{2,1,0:T(8,128)S...) custom-call(bf16[768,2048]{1,0:T(8,128)(2,1)} %latent.1, bf16[768,4096]{1,0:T(8,128)(2,1)} %mix.1, ...), custom_call_target="tpu_custom_call" | custom-call | flops 700000000 | bytes 7000000 | tf_op jit(solution)/shard_map/front/pallas_call | solution.py:196
  11.8 2.1 %collective-permute-start = (f32[8,16,640]{2,1,0:T(8,128)S(1)}, f32[8,16,640]{2,1,0:T(8,128)S(1)}, u32[]{:S(2)}, u32[]{:S(2)}) collective-permute-start(f32[8,16,640]{2,1,0:T(8,128)S(1)} %get-tuple-element.25), channel_id=1, source_target_pairs={{0,32},{1,97},{2,34},{3,99},{4,36},{5,101},{6,38},{7,103},{8,40},{... | collective-permute-start | bytes 983048 | tf_op jit(solution)/shard_map/ppermute | solution.py:385
  17.0 1.8 %collective-permute-start.4 = (f32[8,16,640]{2,1,0:T(8,128)S(1)}, f32[8,16,640]{2,1,0:T(8,128)S(1)}, u32[]{:S(2)}, u32[]{:S(2)}) collective-permute-start(f32[8,16,640]{2,1,0:T(8,128)S(1)} %get-tuple-element.29), channel_id=1, source_target_pairs={{0,34},{1,103},{2,32},{3,101},{4,38},{5,99},{6,36},{7,97},{8,42},{... | collective-permute-start | bytes 983048 | tf_op jit(solution)/shard_map/ppermute | solution.py:385
  18.9 2.6 %collective-permute-start.5 = (f32[8,16,640]{2,1,0:T(8,128)S(1)}, f32[8,16,640]{2,1,0:T(8,128)S(1)}, u32[]{:S(2)}, u32[]{:S(2)}) collective-permute-start(f32[8,16,640]{2,1,0:T(8,128)S(1)} %get-tuple-element.30), channel_id=1, source_target_pairs={{0,10},{1,31},{2,8},{3,29},{4,14},{5,27},{6,12},{7,25},{8,2},{9,23... | collective-permute-start | bytes 983048 | tf_op jit(solution)/shard_map/ppermute | solution.py:385
  21.6 1.7 %collective-permute-start.6 = (f32[8,16,640]{2,1,0:T(8,128)S(1)}, f32[8,16,640]{2,1,0:T(8,128)S(1)}, u32[]{:S(2)}, u32[]{:S(2)}) collective-permute-start(f32[8,16,640]{2,1,0:T(8,128)S(1)} %get-tuple-element.31), channel_id=1, source_target_pairs={{0,42},{1,127},{2,40},{3,125},{4,46},{5,123},{6,44},{7,121},{8,34}... | collective-permute-start | bytes 983048 | tf_op jit(solution)/shard_map/ppermute | solution.py:385
  24.5 3.0 %collective-permute-done.4.refs_5_ = f32[8,16,640]{2,1,0:T(8,128)S(1)} collective-permute-done((f32[8,16,640]{2,1,0:T(8,128)S(1)}, f32[8,16,640]{2,1,0:T(8,128)S(1)}, u32[]{:S(2)}, u32[]{:S(2)}) %collective-permute-start.4) | collective-permute-done | bytes 327712 | tf_op jit(solution)/shard_map/ppermute | solution.py:385
  27.5 4.9 %collective-permute-done.5.refs_6_ = f32[8,16,640]{2,1,0:T(8,128)S(1)} collective-permute-done((f32[8,16,640]{2,1,0:T(8,128)S(1)}, f32[8,16,640]{2,1,0:T(8,128)S(1)}, u32[]{:S(2)}, u32[]{:S(2)}) %collective-permute-start.5) | collective-permute-done | bytes 327712 | tf_op jit(solution)/shard_map/ppermute | solution.py:385
  32.4 3.1 %collective-permute-done.6.refs_7_ = f32[8,16,640]{2,1,0:T(8,128)S(1)} collective-permute-done((f32[8,16,640]{2,1,0:T(8,128)S(1)}, f32[8,16,640]{2,1,0:T(8,128)S(1)}, u32[]{:S(2)}, u32[]{:S(2)}) %collective-permute-start.6) | collective-permute-done | bytes 327712 | tf_op jit(solution)/shard_map/ppermute | solution.py:385
  35.7 2.8 %collective-permute-start.7 = (f32[4,16,640]{2,1,0:T(8,128)S(1)}, f32[4,16,640]{2,1,0:T(8,128)S(1)}, u32[]{:S(2)}, u32[]{:S(2)}) collective-permute-start(f32[4,16,640]{2,1,0:T(8,128)S(1)} %get-tuple-element.32), channel_id=1, source_target_pairs={{0,6},{1,3},{2,4},{3,1},{4,2},{5,7},{6,0},{7,5},{8,14},{9,11},{10,... | collective-permute-start | bytes 491528 | tf_op jit(solution)/shard_map/ppermute | solution.py:385
  38.5 2.2 %collective-permute-start.10 = (f32[4,16,640]{2,1,0:T(8,128)S(1)}, f32[4,16,640]{2,1,0:T(8,128)S(1)}, u32[]{:S(2)}, u32[]{:S(2)}) collective-permute-start(f32[4,16,640]{2,1,0:T(8,128)S(1)} %get-tuple-element.33), channel_id=1, source_target_pairs={{0,24},{1,9},{2,26},{3,11},{4,28},{5,13},{6,30},{7,15},{8,16},{9,1... | collective-permute-start | bytes 491528 | tf_op jit(solution)/shard_map/ppermute | solution.py:385
  40.7 1.6 %collective-permute-done.7 = f32[4,16,640]{2,1,0:T(8,128)S(1)} collective-permute-done((f32[4,16,640]{2,1,0:T(8,128)S(1)}, f32[4,16,640]{2,1,0:T(8,128)S(1)}, u32[]{:S(2)}, u32[]{:S(2)}) %collective-permute-start.7) | collective-permute-done | bytes 163872 | tf_op jit(solution)/shard_map/ppermute | solution.py:385
  42.3 2.3 %collective-permute-start.8 = (f32[4,16,640]{2,1,0:T(8,128)S(1)}, f32[4,16,640]{2,1,0:T(8,128)S(1)}, u32[]{:S(2)}, u32[]{:S(2)}) collective-permute-start(f32[4,16,640]{2,1,0:T(8,128)S(1)} %add.12), channel_id=1, source_target_pairs={{0,24},{1,9},{2,26},{3,11},{4,28},{5,13},{6,30},{7,15},{8,16},{9,1... | collective-permute-start | bytes 491528 | tf_op jit(solution)/shard_map/ppermute | solution.py:385
  45.1 4.1 %collective-permute-start.11 = (f32[4,16,640]{2,1,0:T(8,128)S(1)}, f32[4,16,640]{2,1,0:T(8,128)S(1)}, u32[]{:S(2)}, u32[]{:S(2)}) collective-permute-start(f32[4,16,640]{2,1,0:T(8,128)S(1)} %add.14), channel_id=1, source_target_pairs={{0,96},{1,33},{2,98},{3,35},{4,100},{5,37},{6,102},{7,39},{8,104},... | collective-permute-start | bytes 491528 | tf_op jit(solution)/shard_map/ppermute | solution.py:385
  49.2 3.8 %collective-permute-start.9 = (f32[4,16,640]{2,1,0:T(8,128)S(1)}, f32[4,16,640]{2,1,0:T(8,128)S(1)}, u32[]{:S(2)}, u32[]{:S(2)}) collective-permute-start(f32[4,16,640]{2,1,0:T(8,128)S(1)} %add.13.refs_0_), channel_id=1, source_target_pairs={{0,96},{1,33},{2,98},{3,35},{4,100},{5,37},{6,102},{7,39},{8,104},... | collective-permute-start | bytes 491528 | tf_op jit(solution)/shard_map/ppermute | solution.py:385
  53.1 2.8 %collective-permute-start.12 = (f32[4,16,640]{2,1,0:T(8,128)S(1)}, f32[4,16,640]{2,1,0:T(8,128)S(1)}, u32[]{:S(2)}, u32[]{:S(2)}) collective-permute-start(f32[4,16,640]{2,1,0:T(8,128)S(1)} %add.15.refs_2_), channel_id=1, source_target_pairs={{0,6},{1,3},{2,4},{3,1},{4,2},{5,7},{6,0},{7,5},{8,14},{9,11},{10,... | collective-permute-start | bytes 491528 | tf_op jit(solution)/shard_map/ppermute | solution.py:385
  56.0 2.8 %collective-permute-start.16 = (f32[2,2,16,640]{3,2,1,0:T(8,128)S(1)}, f32[2,2,16,640]{3,2,1,0:T(8,128)S(1)}, u32[]{:S(2)}, u32[]{:S(2)}) collective-permute-start(f32[2,2,16,640]{3,2,1,0:T(8,128)S(1)} %moments.1.refs_0_), channel_id=1, source_target_pairs={{0,120},{1,41},{2,122},{3,43},{4,124},{5,45},{6,126},{7,47},{8,112... | collective-permute-start | bytes 491528 | tf_op jit(solution)/shard_map/ppermute | solution.py:385
  58.7 2.2 %collective-permute-start.15 = (f32[2,2,16,640]{3,2,1,0:T(8,128)S(1)}, f32[2,2,16,640]{3,2,1,0:T(8,128)S(1)}, u32[]{:S(2)}, u32[]{:S(2)}) collective-permute-start(f32[2,2,16,640]{3,2,1,0:T(8,128)S(1)} %moments.1.refs_0_), channel_id=1, source_target_pairs={{0,24},{1,9},{2,26},{3,11},{4,28},{5,13},{6,30},{7,15},{8,16},{9,1... | collective-permute-start | bytes 491528 | tf_op jit(solution)/shard_map/ppermute | solution.py:385
  62.1 8.0 %all_to_all.5.mine = f32[8,2,128]{2,1,0:T(2,128)S(1)} all-to-all(f32[8,2,128]{2,1,0:T(2,128)S(1)} %get-tuple-element.34), channel_id=1, replica_groups={{0,32,8,40,2,34,10,42},{1,97,25,121,7,103,31,127},{3,99,27,123,5,101,29..., dimensions={0} | all-to-all | bytes 16384 | tf_op jit(solution)/shard_map/all_to_all | solution.py:428
  75.6 2.4 %collective-permute-start.19 = (f32[8,16,640]{2,1,0:T(8,128)S(1)}, f32[8,16,640]{2,1,0:T(8,128)S(1)}, u32[]{:S(2)}, u32[]{:S(2)}) collective-permute-start(f32[8,16,640]{2,1,0:T(8,128)S(1)} %direction.1.refs_0_), channel_id=1, source_target_pairs={{0,10},{1,31},{2,8},{3,29},{4,14},{5,27},{6,12},{7,25},{8,2},{9,23... | collective-permute-start | bytes 983048 | tf_op jit(solution)/shard_map/ppermute | solution.py:385
  78.0 1.7 %collective-permute-done.23.refs_3_ = f32[8,16,640]{2,1,0:T(8,128)S(1)} collective-permute-done((f32[8,16,640]{2,1,0:T(8,128)S(1)}, f32[8,16,640]{2,1,0:T(8,128)S(1)}, u32[]{:S(2)}, u32[]{:S(2)}) %collective-permute-start.23) | collective-permute-done | bytes 327712 | tf_op jit(solution)/shard_map/ppermute | solution.py:385
  80.2 9.0 %collective-permute-done.22.refs_2_ = f32[8,16,640]{2,1,0:T(8,128)S(1)} collective-permute-done((f32[8,16,640]{2,1,0:T(8,128)S(1)}, f32[8,16,640]{2,1,0:T(8,128)S(1)}, u32[]{:S(2)}, u32[]{:S(2)}) %collective-permute-start.22) | collective-permute-done | bytes 327712 | tf_op jit(solution)/shard_map/ppermute | solution.py:385
  89.8 2.0 %shard_map.147 = (f32[128,1536]{1,0:T(8,128)}, f32[256,1024]{1,0:T(8,128)}, bf16[128,1536]{1,0:T(8,128)(2,1)}, bf16[256,1024]{1,0:T(8,128)(2,1)}) custom-call(f32[8,16,640]{2,1,0:T(8,128)S(1)} %direction.1.refs_0_, f32[8,16,640]{2,1,0:T(8,128)S(1)} %collective-permute-done.21.refs_1_, f32[8,16,640]{2,1,0:T(8,128)S(1)} %collective-permute-done.22.refs_2_, ...), custom_call_target="tpu_custom_call" | custom-call | flops 200000000 | bytes 2000000 | tf_op jit(solution)/shard_map/pallas_call | solution.py:359
  91.7 4.5 %collective-permute-done.17.refs_0_ = f32[8,16,640]{2,1,0:T(8,128)S(1)} collective-permute-done((f32[8,16,640]{2,1,0:T(8,128)S(1)}, f32[8,16,640]{2,1,0:T(8,128)S(1)}, u32[]{:S(2)}, u32[]{:S(2)}) %collective-permute-start.17) | collective-permute-done | bytes 327712 | tf_op jit(solution)/shard_map/ppermute | solution.py:385
  96.2 1.9 %shard_map.148 = (f32[128,1536]{1,0:T(8,128)}, f32[256,1024]{1,0:T(8,128)}, bf16[128,1536]{1,0:T(8,128)(2,1)}, bf16[256,1024]{1,0:T(8,128)(2,1)}) custom-call(f32[8,16,640]{2,1,0:T(8,128)S(1)} %collective-permute-done.17.refs_0_, ...), custom_call_target="tpu_custom_call", output_to_operand_aliasing={{0}: (8, {}), {1}: (9, {}), {2}: (10, {}), {3}: (11, {})} | custom-call | flops 200000000 | bytes 2000000 | tf_op jit(solution)/shard_map/pallas_call | solution.py:359
  (57 shorter events, 14.5 us)
Async XLA Ops:
  11.8 7.2 %collective-permute-start = (f32[8,16,640]{2,1,0:T(8,128)S(1)}, f32[8,16,640]{2,1,0:T(8,128)S(1)}, u32[]{:S(2)}, u32[]{:S(2)}) collective-permute-start(f32[8,16,640]{2,1,0:T(8,128)S(1)} %get-tuple-element.25), channel_id=1, source_target_pairs={{0,32},{1,97},{2,34},{3,99},{4,36},{5,101},{6,38},{7,103},{8,40},{... | collective-permute-start | bytes 983048 | tf_op jit(solution)/shard_map/ppermute | solution.py:385
  13.9 7.7 %collective-permute-start.1 = (f32[8,16,640]{2,1,0:T(8,128)S(1)}, f32[8,16,640]{2,1,0:T(8,128)S(1)}, u32[]{:S(2)}, u32[]{:S(2)}) collective-permute-start(f32[8,16,640]{2,1,0:T(8,128)S(1)} %get-tuple-element.26), channel_id=1, source_target_pairs={{0,8},{1,25},{2,10},{3,27},{4,12},{5,29},{6,14},{7,31},{8,0},{9,17... | collective-permute-start | bytes 983048 | tf_op jit(solution)/shard_map/ppermute | solution.py:385
  15.5 9.0 %collective-permute-start.2 = (f32[8,16,640]{2,1,0:T(8,128)S(1)}, f32[8,16,640]{2,1,0:T(8,128)S(1)}, u32[]{:S(2)}, u32[]{:S(2)}) collective-permute-start(f32[8,16,640]{2,1,0:T(8,128)S(1)} %get-tuple-element.27), channel_id=1, source_target_pairs={{0,40},{1,121},{2,42},{3,123},{4,44},{5,125},{6,46},{7,127},{8,32}... | collective-permute-start | bytes 983048 | tf_op jit(solution)/shard_map/ppermute | solution.py:385
  15.5 9.0 %collective-permute-start.3 = (f32[8,16,640]{2,1,0:T(8,128)S(1)}, f32[8,16,640]{2,1,0:T(8,128)S(1)}, u32[]{:S(2)}, u32[]{:S(2)}) collective-permute-start(f32[8,16,640]{2,1,0:T(8,128)S(1)} %get-tuple-element.28), channel_id=1, source_target_pairs={{0,2},{1,7},{2,0},{3,5},{4,6},{5,3},{6,4},{7,1},{8,10},{9,15},{10,... | collective-permute-start | bytes 983048 | tf_op jit(solution)/shard_map/ppermute | solution.py:385
  17.0 10.5 %collective-permute-start.4 = (f32[8,16,640]{2,1,0:T(8,128)S(1)}, f32[8,16,640]{2,1,0:T(8,128)S(1)}, u32[]{:S(2)}, u32[]{:S(2)}) collective-permute-start(f32[8,16,640]{2,1,0:T(8,128)S(1)} %get-tuple-element.29), channel_id=1, source_target_pairs={{0,34},{1,103},{2,32},{3,101},{4,38},{5,99},{6,36},{7,97},{8,42},{... | collective-permute-start | bytes 983048 | tf_op jit(solution)/shard_map/ppermute | solution.py:385
  18.9 13.5 %collective-permute-start.5 = (f32[8,16,640]{2,1,0:T(8,128)S(1)}, f32[8,16,640]{2,1,0:T(8,128)S(1)}, u32[]{:S(2)}, u32[]{:S(2)}) collective-permute-start(f32[8,16,640]{2,1,0:T(8,128)S(1)} %get-tuple-element.30), channel_id=1, source_target_pairs={{0,10},{1,31},{2,8},{3,29},{4,14},{5,27},{6,12},{7,25},{8,2},{9,23... | collective-permute-start | bytes 983048 | tf_op jit(solution)/shard_map/ppermute | solution.py:385
  21.6 13.9 %collective-permute-start.6 = (f32[8,16,640]{2,1,0:T(8,128)S(1)}, f32[8,16,640]{2,1,0:T(8,128)S(1)}, u32[]{:S(2)}, u32[]{:S(2)}) collective-permute-start(f32[8,16,640]{2,1,0:T(8,128)S(1)} %get-tuple-element.31), channel_id=1, source_target_pairs={{0,42},{1,127},{2,40},{3,125},{4,46},{5,123},{6,44},{7,121},{8,34}... | collective-permute-start | bytes 983048 | tf_op jit(solution)/shard_map/ppermute | solution.py:385
  35.7 6.6 %collective-permute-start.7 = (f32[4,16,640]{2,1,0:T(8,128)S(1)}, f32[4,16,640]{2,1,0:T(8,128)S(1)}, u32[]{:S(2)}, u32[]{:S(2)}) collective-permute-start(f32[4,16,640]{2,1,0:T(8,128)S(1)} %get-tuple-element.32), channel_id=1, source_target_pairs={{0,6},{1,3},{2,4},{3,1},{4,2},{5,7},{6,0},{7,5},{8,14},{9,11},{10,... | collective-permute-start | bytes 491528 | tf_op jit(solution)/shard_map/ppermute | solution.py:385
  38.5 6.5 %collective-permute-start.10 = (f32[4,16,640]{2,1,0:T(8,128)S(1)}, f32[4,16,640]{2,1,0:T(8,128)S(1)}, u32[]{:S(2)}, u32[]{:S(2)}) collective-permute-start(f32[4,16,640]{2,1,0:T(8,128)S(1)} %get-tuple-element.33), channel_id=1, source_target_pairs={{0,24},{1,9},{2,26},{3,11},{4,28},{5,13},{6,30},{7,15},{8,16},{9,1... | collective-permute-start | bytes 491528 | tf_op jit(solution)/shard_map/ppermute | solution.py:385
  42.3 6.9 %collective-permute-start.8 = (f32[4,16,640]{2,1,0:T(8,128)S(1)}, f32[4,16,640]{2,1,0:T(8,128)S(1)}, u32[]{:S(2)}, u32[]{:S(2)}) collective-permute-start(f32[4,16,640]{2,1,0:T(8,128)S(1)} %add.12), channel_id=1, source_target_pairs={{0,24},{1,9},{2,26},{3,11},{4,28},{5,13},{6,30},{7,15},{8,16},{9,1... | collective-permute-start | bytes 491528 | tf_op jit(solution)/shard_map/ppermute | solution.py:385
  45.1 8.0 %collective-permute-start.11 = (f32[4,16,640]{2,1,0:T(8,128)S(1)}, f32[4,16,640]{2,1,0:T(8,128)S(1)}, u32[]{:S(2)}, u32[]{:S(2)}) collective-permute-start(f32[4,16,640]{2,1,0:T(8,128)S(1)} %add.14), channel_id=1, source_target_pairs={{0,96},{1,33},{2,98},{3,35},{4,100},{5,37},{6,102},{7,39},{8,104},... | collective-permute-start | bytes 491528 | tf_op jit(solution)/shard_map/ppermute | solution.py:385
  49.2 12.8 %collective-permute-start.9 = (f32[4,16,640]{2,1,0:T(8,128)S(1)}, f32[4,16,640]{2,1,0:T(8,128)S(1)}, u32[]{:S(2)}, u32[]{:S(2)}) collective-permute-start(f32[4,16,640]{2,1,0:T(8,128)S(1)} %add.13.refs_0_), channel_id=1, source_target_pairs={{0,96},{1,33},{2,98},{3,35},{4,100},{5,37},{6,102},{7,39},{8,104},... | collective-permute-start | bytes 491528 | tf_op jit(solution)/shard_map/ppermute | solution.py:385
  53.1 8.9 %collective-permute-start.12 = (f32[4,16,640]{2,1,0:T(8,128)S(1)}, f32[4,16,640]{2,1,0:T(8,128)S(1)}, u32[]{:S(2)}, u32[]{:S(2)}) collective-permute-start(f32[4,16,640]{2,1,0:T(8,128)S(1)} %add.15.refs_2_), channel_id=1, source_target_pairs={{0,6},{1,3},{2,4},{3,1},{4,2},{5,7},{6,0},{7,5},{8,14},{9,11},{10,... | collective-permute-start | bytes 491528 | tf_op jit(solution)/shard_map/ppermute | solution.py:385
  56.0 14.0 %collective-permute-start.16 = (f32[2,2,16,640]{3,2,1,0:T(8,128)S(1)}, f32[2,2,16,640]{3,2,1,0:T(8,128)S(1)}, u32[]{:S(2)}, u32[]{:S(2)}) collective-permute-start(f32[2,2,16,640]{3,2,1,0:T(8,128)S(1)} %moments.1.refs_0_), channel_id=1, source_target_pairs={{0,120},{1,41},{2,122},{3,43},{4,124},{5,45},{6,126},{7,47},{8,112... | collective-permute-start | bytes 491528 | tf_op jit(solution)/shard_map/ppermute | solution.py:385
  58.7 11.3 %collective-permute-start.15 = (f32[2,2,16,640]{3,2,1,0:T(8,128)S(1)}, f32[2,2,16,640]{3,2,1,0:T(8,128)S(1)}, u32[]{:S(2)}, u32[]{:S(2)}) collective-permute-start(f32[2,2,16,640]{3,2,1,0:T(8,128)S(1)} %moments.1.refs_0_), channel_id=1, source_target_pairs={{0,24},{1,9},{2,26},{3,11},{4,28},{5,13},{6,30},{7,15},{8,16},{9,1... | collective-permute-start | bytes 491528 | tf_op jit(solution)/shard_map/ppermute | solution.py:385
  60.9 9.1 %collective-permute-start.14 = (f32[2,2,16,640]{3,2,1,0:T(8,128)S(1)}, f32[2,2,16,640]{3,2,1,0:T(8,128)S(1)}, u32[]{:S(2)}, u32[]{:S(2)}) collective-permute-start(f32[2,2,16,640]{3,2,1,0:T(8,128)S(1)} %moments.1.refs_0_), channel_id=1, source_target_pairs={{0,96},{1,33},{2,98},{3,35},{4,100},{5,37},{6,102},{7,39},{8,104},... | collective-permute-start | bytes 491528 | tf_op jit(solution)/shard_map/ppermute | solution.py:385
  70.0 1.2 %collective-permute-start.13 = (f32[8,2,128]{2,1,0:T(2,128)S(1)}, f32[8,2,128]{2,1,0:T(2,128)S(1)}, u32[]{:S(2)}, u32[]{:S(2)}) collective-permute-start(f32[8,2,128]{2,1,0:T(2,128)S(1)} %all_to_all.5.mine), channel_id=1, source_target_pairs={{0,1},{1,0},{2,3},{3,2},{4,5},{5,4},{6,7},{7,6},{8,9},{9,8},{10,11... | collective-permute-start | bytes 24584 | tf_op jit(solution)/shard_map/ppermute | solution.py:429
  71.5 8.2 %collective-permute-start.23 = (f32[8,16,640]{2,1,0:T(8,128)S(1)}, f32[8,16,640]{2,1,0:T(8,128)S(1)}, u32[]{:S(2)}, u32[]{:S(2)}) collective-permute-start(f32[8,16,640]{2,1,0:T(8,128)S(1)} %direction.1.refs_0_), channel_id=1, source_target_pairs={{0,40},{1,121},{2,42},{3,123},{4,44},{5,125},{6,46},{7,127},{8,32}... | collective-permute-start | bytes 983048 | tf_op jit(solution)/shard_map/ppermute | solution.py:385
  72.1 17.0 %collective-permute-start.22 = (f32[8,16,640]{2,1,0:T(8,128)S(1)}, f32[8,16,640]{2,1,0:T(8,128)S(1)}, u32[]{:S(2)}, u32[]{:S(2)}) collective-permute-start(f32[8,16,640]{2,1,0:T(8,128)S(1)} %direction.1.refs_0_), channel_id=1, source_target_pairs={{0,8},{1,25},{2,10},{3,27},{4,12},{5,29},{6,14},{7,31},{8,0},{9,17... | collective-permute-start | bytes 983048 | tf_op jit(solution)/shard_map/ppermute | solution.py:385
  73.6 16.2 %collective-permute-start.21 = (f32[8,16,640]{2,1,0:T(8,128)S(1)}, f32[8,16,640]{2,1,0:T(8,128)S(1)}, u32[]{:S(2)}, u32[]{:S(2)}) collective-permute-start(f32[8,16,640]{2,1,0:T(8,128)S(1)} %direction.1.refs_0_), channel_id=1, source_target_pairs={{0,32},{1,97},{2,34},{3,99},{4,36},{5,101},{6,38},{7,103},{8,40},{... | collective-permute-start | bytes 983048 | tf_op jit(solution)/shard_map/ppermute | solution.py:385
  75.1 16.7 %collective-permute-start.20 = (f32[8,16,640]{2,1,0:T(8,128)S(1)}, f32[8,16,640]{2,1,0:T(8,128)S(1)}, u32[]{:S(2)}, u32[]{:S(2)}) collective-permute-start(f32[8,16,640]{2,1,0:T(8,128)S(1)} %direction.1.refs_0_), channel_id=1, source_target_pairs={{0,42},{1,127},{2,40},{3,125},{4,46},{5,123},{6,44},{7,121},{8,34}... | collective-permute-start | bytes 983048 | tf_op jit(solution)/shard_map/ppermute | solution.py:385
  75.6 16.1 %collective-permute-start.19 = (f32[8,16,640]{2,1,0:T(8,128)S(1)}, f32[8,16,640]{2,1,0:T(8,128)S(1)}, u32[]{:S(2)}, u32[]{:S(2)}) collective-permute-start(f32[8,16,640]{2,1,0:T(8,128)S(1)} %direction.1.refs_0_), channel_id=1, source_target_pairs={{0,10},{1,31},{2,8},{3,29},{4,14},{5,27},{6,12},{7,25},{8,2},{9,23... | collective-permute-start | bytes 983048 | tf_op jit(solution)/shard_map/ppermute | solution.py:385
  79.6 12.1 %collective-permute-start.18 = (f32[8,16,640]{2,1,0:T(8,128)S(1)}, f32[8,16,640]{2,1,0:T(8,128)S(1)}, u32[]{:S(2)}, u32[]{:S(2)}) collective-permute-start(f32[8,16,640]{2,1,0:T(8,128)S(1)} %direction.1.refs_0_), channel_id=1, source_target_pairs={{0,34},{1,103},{2,32},{3,101},{4,38},{5,99},{6,36},{7,97},{8,42},{... | collective-permute-start | bytes 983048 | tf_op jit(solution)/shard_map/ppermute | solution.py:385
  89.2 7.1 %collective-permute-start.17 = (f32[8,16,640]{2,1,0:T(8,128)S(1)}, f32[8,16,640]{2,1,0:T(8,128)S(1)}, u32[]{:S(2)}, u32[]{:S(2)}) collective-permute-start(f32[8,16,640]{2,1,0:T(8,128)S(1)} %direction.1.refs_0_), channel_id=1, source_target_pairs={{0,2},{1,7},{2,0},{3,5},{4,6},{5,3},{6,4},{7,1},{8,10},{9,15},{10,... | collective-permute-start | bytes 983048 | tf_op jit(solution)/shard_map/ppermute | solution.py:385
  (10 other events, 412.5 us)
